TPU v7x, 256 devices: a whole 4x4x8 slice. The times are simulated.
256 devices in a mesh: sp: 32 (over z, y), tp: 8 (over x, core).
Axes of the slice: x: 4, y: 4, z: 8, core: 2. Of those that a mesh axis runs over, the one named last changes fastest.
Arguments:
- tokens: bfloat16 [4, 16384, 2048], P(None, ('sp', 'tp')), may hold values from -6 to 6
- in_gain: float32 [2048], replicated, may hold values from 0.1 to 1.9
- query_weight: bfloat16 [2048, 1024], P(None, 'tp'), may hold values from -0.125 to 0.125
- key_weight: bfloat16 [2048, 1024], P(None, 'tp'), may hold values from -0.125 to 0.125
- value_weight: bfloat16 [2048, 1024], P(None, 'tp'), may hold values from -0.125 to 0.125
- gate_weight: bfloat16 [2048, 1024], P(None, 'tp'), may hold values from -0.125 to 0.125
- log_decay: float32 [8], P('tp'), may hold values from -0.034 to 0, as said below
- norm_gain: float32 [1024], P('tp'), may hold values from 0.1 to 1.9
- out_weight: bfloat16 [1024, 2048], replicated, may hold values from -0.1875 to 0.1875
- post_gain: float32 [2048], replicated, may hold values from 0.1 to 1.9
Outputs:
- mixed: bfloat16 [4, 16384, 2048], P(None, ('sp', 'tp'))
Inputs may be any that keep to these rules, and one draw needn't show every extreme that they name: `log_decay`: every entry is negative; some heads keep a tenth or more of their memory over 16384 positions, others lose most of it within 30 to 100 positions.
All inputs are finite; a program needn't handle non-finite values.
Results may differ from a plain program's by a relative error of at most 0.015.
Values may be sent and summed in bfloat16 or wider, within the bound.
A program may use at most 64 MiB of HBM per device.

v0:
```python
import jax
import jax.numpy as jnp
from jax import lax
from jax.sharding import Mesh
from jax.sharding import PartitionSpec as P

HEAD_DIM = 128
BLOCK = 128
SP = ("sp_0", "sp_1")
SP_TP = ("sp_0", "sp_1", "tp")
rms_eps = 1e-06
group_eps = 1e-05
rope_base = 10000.0


def neutral_like(shard, identity):
    return jax.tree.map(
        lambda part, zero: jnp.zeros_like(part) + jnp.asarray(zero, part.dtype), shard, identity
    )


def entering(shard, axes, combine, identity):
    before = start = neutral_like(shard, identity)
    running = shard
    for axis in reversed(axes):
        length, mine = (lax.axis_size(axis), lax.axis_index(axis))
        pieces = jax.tree.map(lambda part: lax.all_gather(part, axis), running)
        inside, running = (start, start)
        for k in range(length):
            passed = k < mine
            running = combine(running, jax.tree.map(lambda part: part[k], pieces))
            inside = jax.tree.map(lambda new, old: jnp.where(passed, new, old), running, inside)
        before = combine(inside, before)
    return before


def rotate(values, positions):
    half_dim = values.shape[-1] // 2
    inverse = rope_base ** (-jnp.arange(half_dim, dtype=jnp.float32) / half_dim)
    angles = positions.astype(jnp.float32)[:, None] * inverse[None, :]
    cosine = jnp.cos(angles)
    sine_part = jnp.sin(angles)
    first_half = values[..., :half_dim].astype(jnp.float32)
    second = values[..., half_dim:].astype(jnp.float32)
    return jnp.concatenate(
        [first_half * cosine - second * sine_part, first_half * sine_part + second * cosine],
        axis=-1,
    )


def local_pass(queries, key_rows, values, log_decay):
    seq_count, head_count, length, head_width = queries.shape
    block_count = length // BLOCK
    offsets = jnp.arange(BLOCK, dtype=jnp.float32)
    distance = offsets[:, None] - offsets[None, :]
    rate_col = log_decay[:, None, None]
    inside = jnp.where(distance >= 0, jnp.exp(rate_col * jnp.maximum(distance, 0.0)), 0.0)
    query_scale = jnp.exp(log_decay[:, None] * (offsets + 1.0))[..., None]
    key_scale = jnp.exp(log_decay[:, None] * (BLOCK - 1.0 - offsets))[..., None]
    block_decay = jnp.exp(log_decay * BLOCK)[:, None, None]

    def to_blocks(arr):
        return arr.reshape(seq_count, head_count, block_count, BLOCK, arr.shape[-1]).transpose(
            2, 0, 1, 3, 4
        )

    def advance(memory, inputs):
        q_block, k_block, v_block = inputs
        scores = jnp.einsum("shqd,shkd->shqk", q_block, k_block, preferred_element_type=jnp.float32)
        weights = (scores * inside).astype(jnp.bfloat16)
        within = jnp.einsum("shqk,shkv->shqv", weights, v_block, preferred_element_type=jnp.float32)
        carried = jnp.einsum("shqd,shdv->shqv", q_block.astype(jnp.float32) * query_scale, memory)
        k_scaled = (k_block.astype(jnp.float32) * key_scale).astype(jnp.bfloat16)
        memory = memory * block_decay + jnp.einsum(
            "shkd,shkv->shdv", k_scaled, v_block, preferred_element_type=jnp.float32
        )
        return (memory, within + carried)

    start_memory = jnp.zeros((seq_count, head_count, head_width, values.shape[-1]), jnp.float32)
    end_state, outputs = lax.scan(
        advance, start_memory, (to_blocks(queries), to_blocks(key_rows), to_blocks(values))
    )
    outputs = outputs.transpose(1, 2, 0, 3, 4).reshape(
        seq_count, head_count, length, values.shape[-1]
    )
    return (outputs, end_state)


def combine(earlier, later_part):
    return (
        earlier[0] * later_part[0],
        earlier[1] * later_part[0][None, :, None, None] + later_part[1],
    )


def read_out(carried, queries, partial_out, log_decay):
    length = queries.shape[2]
    read_scale = jnp.exp(log_decay[:, None] * (jnp.arange(length, dtype=jnp.float32) + 1.0))[
        ..., None
    ]
    return partial_out + jnp.einsum(
        "shld,shdv->shlv", queries.astype(jnp.float32) * read_scale, carried
    )


def body(
    tokens,
    in_gain,
    query_weight,
    key_weight,
    value_weight,
    gate_weight,
    log_decay,
    norm_gain,
    out_weight,
    post_gain,
):
    seq_count, rows_dev, model_width = tokens.shape
    tp_size = lax.axis_size("tp")
    local_width = query_weight.shape[1]
    head_count = local_width // HEAD_DIM
    stretch = rows_dev * tp_size
    tok_f32 = tokens.astype(jnp.float32)
    normed = (
        tok_f32 * lax.rsqrt(jnp.mean(tok_f32 * tok_f32, axis=-1, keepdims=True) + rms_eps) * in_gain
    ).astype(jnp.bfloat16)
    joined = jnp.concatenate([query_weight, key_weight, value_weight, gate_weight], axis=1)
    projected = jnp.einsum(
        "kux,xt->kut",
        lax.all_gather(normed, "tp", axis=1, tiled=True),
        joined,
        preferred_element_type=jnp.float32,
    ).astype(jnp.bfloat16)

    def heads_of(columns):
        return columns.reshape(seq_count, stretch, head_count, HEAD_DIM).transpose(0, 2, 1, 3)

    positions = lax.axis_index(SP) * stretch + jnp.arange(stretch, dtype=jnp.int32)
    queries = rotate(heads_of(projected[..., :local_width]), positions).astype(jnp.bfloat16)
    key_rows = (
        rotate(heads_of(projected[..., local_width : 2 * local_width]), positions)
        * HEAD_DIM ** (-0.5)
    ).astype(jnp.bfloat16)
    values = heads_of(projected[..., 2 * local_width : 3 * local_width])
    gating = projected[..., 3 * local_width :]
    partial_out, end_state = local_pass(queries, key_rows, values, log_decay)
    span_decay = jnp.exp(log_decay * stretch)
    carried = entering(
        (span_decay, end_state), SP, combine, (jnp.ones_like(span_decay), jnp.zeros_like(end_state))
    )[1]
    retained = read_out(carried, queries, partial_out, log_decay)
    center = jnp.mean(retained, axis=-1, keepdims=True)
    spread = jnp.mean(jnp.square(retained - center), axis=-1, keepdims=True)
    normal = (
        ((retained - center) * lax.rsqrt(spread + group_eps))
        .transpose(0, 2, 1, 3)
        .reshape(seq_count, stretch, local_width)
    )
    gated = (normal * norm_gain * jax.nn.silu(gating.astype(jnp.float32))).astype(jnp.bfloat16)
    premix = jnp.einsum(
        "hor,rn->hon",
        lax.all_to_all(gated, "tp", split_axis=1, concat_axis=2, tiled=True),
        out_weight,
        preferred_element_type=jnp.float32,
    )
    mixed = (
        premix * lax.rsqrt(jnp.mean(premix * premix, axis=-1, keepdims=True) + rms_eps) * post_gain
    )
    return mixed.astype(jnp.bfloat16)


def solution(mesh):
    torus = Mesh(mesh.devices.reshape(8, 4, mesh.shape["tp"]), ("sp_0", "sp_1", "tp"))
    return jax.shard_map(
        body,
        mesh=torus,
        in_specs=(
            P(None, SP_TP, None),
            P(),
            P(None, "tp"),
            P(None, "tp"),
            P(None, "tp"),
            P(None, "tp"),
            P("tp"),
            P("tp"),
            P(),
            P(),
        ),
        out_specs=P(None, SP_TP, None),
        check_vma=False,
    )
```

profile of v0, /device:TPU:1, one launch (start us, length us, event | category | flops | bytes accessed | tf_op | source)
XLA Modules:
  0.0 204.7 jit_solution(9332395953188734523)
XLA Ops:
  6.5 1.6 fusion.44
  8.1 2.6 %fusion.46 = bf16[4,64,2048]{2,1,0:T(8,128)(2,1)} fusion(bf16[4,64,2048]{2,1,0:T(8,128)(2,1)} %param.12, f32[2048]{0:T(1024)} %param.13, f32[4,64]{1,0:T(4,128)S(1)} %add_rsqrt_fusion.2), kind=kLoop, calls=%fused_computation.48 | loop fusion | flops 2097152 | bytes 2106368 | tf_op jit(solution)/shard_map/convert_element_type | solution.py:126
  13.5 53.8 %all-gather.7.cloned.1.call-done = bf16[4,512,2048]{2,1,0:T(8,128)(2,1)} async-done(((bf16[4,64,2048]{2,1,0:T(8,128)(2,1)}), bf16[4,512,2048]{2,1,0:T(8,128)(2,1)}) %all-gather.7.cloned.1.call-update) | async-done | bytes 8388624 | tf_op jit(solution)/shard_map/all_gather | solution.py:130
  67.3 9.5 %fusion.54 = bf16[4,512,512]{1,2,0:T(8,128)(2,1)S(1)} fusion(bf16[4,512,2048]{2,1,0:T(8,128)(2,1)} %all-gather.7.cloned.1.call-done, bf16[2048,128]{0,1:T(8,128)(2,1)S(1)} %copy.42, bf16[2048,128]{0,1:T(8,128)(2,1)S(1)} %copy.41, bf16[2048,128]{0,1:T(8,128)(2,1)S(1)} %copy.40, bf16[2048,128]{0,1:T(8,128)(2,1)S(1)} %copy.39), kind=kOutput, calls=%fused_computation.59 | convolution fusion | flops 4304404480 | bytes 12582912 | tf_op jit(solution)/shard_map/kux,xt->kut/dot_general | solution.py:128
  76.9 1.0 slice_bitcast_fusion
  80.3 1.3 copy.44
  81.6 1.2 reshape_transpose_reshape.3
  84.8 11.9 %while.15 = (s32[]{:T(128)}, f32[4,1,128,128]{3,2,0,1:T(8,128)S(1)}, f32[4,4,1,128,128]{4,3,1,2,0:T(8,128)}, f32[1]{0:T(128)}, bf16[4,4,1,128,128]{4,3,1,2,0:T(8...) while((s32[]{:T(128)}, ...), condition=%wide.region_2.3_spmd.clone.clone.clone, body=%wide.region_1.2_spmd.clone.clone.clone.sunk | while | flops 67977728 | bytes 2496632 | solution.py:80
  86.5 0.9 fusion.147
  89.5 0.9 fusion.147
  92.5 0.9 fusion.147
  95.5 0.9 fusion.147
  98.8 8.4 %all-reduce = f32[4]{0:T(128)S(1)} all-reduce(f32[4]{0:T(128)S(1)} %exponential_dynamic-update-slice_fusion), channel_id=2, replica_groups=mesh['sp_0'=8,'sp_1'=4,'tp'=8] {'sp_1'}, use_global_device_ids=true, to_apply=%add | all-reduce | flops 4 | bytes 32
  107.9 1.3 slice_multiply_fusion
  109.9 12.2 %all-gather.11.cloned.1.call-done = f32[16,1,128,128]{3,2,1,0:T(8,128)} async-done(((f32[4,1,128,128]{3,2,1,0:T(8,128)}), f32[16,1,128,128]{3,2,1,0:T(8,128)}) %all-gather.11.cloned.1.call-update) | async-done | bytes 1048592 | tf_op jit(solution)/shard_map/all_gather | solution.py:27
  122.0 3.8 %slice_add_fusion.8 = f32[4,1,128,128]{3,2,1,0:T(8,128)} fusion(f32[16,1,128,128]{3,2,1,0:T(8,128)} %all-gather.11.cloned.1.call-done, f32[]{:T(128)} %bitcast.20, f32[]{:T(128)} %bitcast.18, f32[16,1,128,128]{3,2,0,1:T(8,128)} %bitcast.197, f32[]{:T(128)} %bitcast.16, f32[]{:T(128)} %bitcast.13), kind=kLoop, calls=%fused_computation.109 | loop fusion | flops 458752 | bytes 1310736 | tf_op jit(solution)/shard_map/add | solution.py:92
  126.4 1.3 dynamic-update-slice.1
  127.7 13.9 %all-reduce.1 = f32[8]{0:T(128)S(1)} all-reduce(f32[8]{0:T(128)S(1)} %dynamic-update-slice.1), channel_id=3, replica_groups=mesh['sp_0'=8,'sp_1'=4,'tp'=8] {'sp_0'}, use_global_device_ids=true, to_apply=%add.1 | all-reduce | flops 8 | bytes 64
  146.3 18.7 %all-gather.9.cloned.1.call-done = f32[8,4,1,128,128]{4,3,2,1,0:T(8,128)} async-done(((f32[1,4,1,128,128]{4,3,2,1,0:T(8,128)}), f32[8,4,1,128,128]{4,3,2,1,0:T(8,128)}) %all-gather.9.cloned.1.call-update) | async-done | bytes 2097168 | tf_op jit(solution)/shard_map/all_gather | solution.py:27
  165.1 7.9 %fusion.128 = (f32[4,512]{1,0:T(4,128)S(1)}, f32[4,512,128]{1,2,0:T(8,128)S(1)}) fusion(f32[4,512,128]{1,2,0:T(8,128)S(1)} %reshape.499, f32[8,4,1,128,128]{4,3,1,2,0:T(8,128)} %bitcast.204, f32[4,1,128,128]{3,2,1,0:T(8,128)S(1)} %copy-done.4, f32[16,1,128,128]{3,2,0,1:T(8,128)S(1)} %bitcast.198, f32[16,1,128,128]{3,2,1,0:T(8,128)S(1)} %copy-done.3, ...), kind=kOutput, calls=%fused_computation.175 | convolution fusion | flops 71170048 | bytes 5777468 | tf_op jit(solution)/shard_map/shld,shdv->shlv/dot_general | solution.py:101
  173.2 1.5 fusion.62
  175.0 18.3 %all_to_all.18 = bf16[4,512,128]{2,0,1:T(4,128)(2,1)S(1)} all-to-all(bf16[4,512,128]{2,0,1:T(4,128)(2,1)S(1)} %copy.65), channel_id=1, replica_groups=mesh['sp_0'=8,'sp_1'=4,'tp'=8] {'tp'}, dimensions={1} | all-to-all | bytes 1048576 | tf_op jit(solution)/shard_map/all_to_all | solution.py:162
  193.4 3.6 %multiply_reduce_fusion = (f32[4,64]{1,0:T(4,128)S(1)}, f32[4,64,2048]{2,1,0:T(8,128)S(1)}) fusion(bf16[1024,2048]{1,0:T(8,128)(2,1)} %param.20, bf16[4,8,8,8,128]{4,3,2,1,0:T(8,128)(2,1)S(1)} %bitcast.203), kind=kOutput, calls=%fused_computation.58 | convolution fusion | flops 1074790144 | bytes 6816768 | tf_op jit(solution)/shard_map/hor,rn->hon/dot_general | solution.py:160
  197.0 1.2 multiply_convert_fusion.2
  (91 shorter events, 19.6 us)
Async XLA Ops:
  6.5 4.3 %copy-start.8 = (bf16[2048,128]{1,0:T(8,128)(2,1)S(1)}, bf16[2048,128]{1,0:T(8,128)(2,1)}, u32[]{:S(2)}) copy-start(bf16[2048,128]{1,0:T(8,128)(2,1)} %param.14) | copy-start | bytes 1572868
  6.5 60.8 %all-gather.7.cloned.1.call-start = ((), (), s32[]{:S(2)}) async-start(), calls=%async_computation.1 | async-start | bytes 9437184 | tf_op jit(solution)/shard_map/all_gather | solution.py:130
  8.1 3.0 %copy-start.9 = (bf16[2048,128]{1,0:T(8,128)(2,1)S(1)}, bf16[2048,128]{1,0:T(8,128)(2,1)}, u32[]{:S(2)}) copy-start(bf16[2048,128]{1,0:T(8,128)(2,1)} %param.15) | copy-start | bytes 1572868
  10.8 1.0 copy-start.10
  10.8 1.3 copy-start.11
  10.8 111.2 %all-gather.11.cloned.1.call-start = ((), (), s32[]{:S(2)}) async-start(), calls=%async_computation.3 | async-start | bytes 1310720 | tf_op jit(solution)/shard_map/all_gather | solution.py:27
  76.9 1.5 copy-start.2
  78.3 0.7 copy-start.6
  78.4 0.8 copy-start.7
  83.2 1.2 copy-start.1
  84.8 12.8 %copy-start.15 = (u32[256]{0:T(256)S(1)}, u32[256]{0:T(256)}, u32[]{:S(2)}) copy-start(u32[256]{0:T(256)} %constant.86) | copy-start | bytes 3076
  84.8 41.1 %copy-start.14 = (u32[256]{0:T(256)S(1)}, u32[256]{0:T(256)}, u32[]{:S(2)}) copy-start(u32[256]{0:T(256)} %constant.91) | copy-start | bytes 3076
  96.7 0.7 copy-start
  96.7 48.7 %copy-start.5 = (f32[4,4,1,128,128]{4,3,1,2,0:T(8,128)S(1)}, f32[4,4,1,128,128]{4,3,1,2,0:T(8,128)}, u32[]{:S(2)}) copy-start(f32[4,4,1,128,128]{4,3,1,2,0:T(8,128)} %get-tuple-element.58) | copy-start | bytes 3145732
  97.5 67.6 %all-gather.9.cloned.1.call-start = ((), (), s32[]{:S(2)}) async-start(), calls=%async_computation.2 | async-start | bytes 2359296 | tf_op jit(solution)/shard_map/all_gather | solution.py:27
  145.5 19.6 %copy-start.3 = (f32[16,1,128,128]{3,2,1,0:T(8,128)S(1)}, f32[16,1,128,128]{3,2,1,0:T(8,128)}, u32[]{:S(2)}) copy-start(f32[16,1,128,128]{3,2,1,0:T(8,128)} %all-gather.11.cloned.1.call-done) | copy-start | bytes 3145732
  145.5 19.6 %copy-start.4 = (f32[4,1,128,128]{3,2,1,0:T(8,128)S(1)}, f32[4,1,128,128]{3,2,1,0:T(8,128)}, u32[]{:S(2)}) copy-start(f32[4,1,128,128]{3,2,1,0:T(8,128)} %slice_add_fusion.8) | copy-start | bytes 786436
  165.1 8.1 %copy-start.13 = (f32[128]{0:T(128)S(1)}, f32[128]{0:T(128)}, u32[]{:S(2)}) copy-start(f32[128]{0:T(128)} %param.19) | copy-start | bytes 1540
  193.4 3.6 %copy-start.12 = (f32[2048]{0:T(1024)S(1)}, f32[2048]{0:T(1024)}, u32[]{:S(2)}) copy-start(f32[2048]{0:T(1024)} %param.21) | copy-start | bytes 24580
Sparse Core Ops, SparseCore 0:
  10.9 56.3 all-gather.6
  97.6 24.3 all-gather.10
  126.0 39.0 all-gather.8
where the time goes:
time: 205 us
  waiting for transfers between devices  84.8 us (41%)
  blocking collectives  40.6 us (20%)
  matrix products  27.4 us (13%)
  other arithmetic  20.4 us (10%)
  between operations  18 us (9%)
  local copies, waits for them, and re-layouts  13.3 us (6%)
    all_gather x1, waiting for transfers between devices, body(): lax.all_gather(normed, 'tp', axis=1, tiled=True)  53.8 us
    all_gather x2, waiting for transfers between devices, entering(): pieces = jax.tree.map(lambda part: lax.all_gather(part, axis), running)  30.9 us
    unnamed x2, blocking collectives  22.3 us
    all_to_all x1, blocking collectives, body(): lax.all_to_all(gated, 'tp', split_axis=1, concat_axis=2, tiled=True)  18.3 us
    dot_general x1, matrix products, body(): jnp.einsum('kux,xt->kut', lax.all_gather(normed, 'tp', axis=1, tiled=True...  9.51 us
    dot_general x1, matrix products, read_out(): jnp.einsum('shld,shdv->shlv', queries.astype(jnp.float32) * read_scale, c...  7.93 us
    unnamed x41, local copies, waits for them, and re-layouts  6.03 us
  transfers between devices with their start and end apart: 3, of which 3 were waited for; matrix products, arithmetic and copies ran while one was open for 4% of the time, Pallas kernels for 0%

commit v1 on v0

--- a/solution.py
+++ b/solution.py
@@ -11,6 +11,30 @@
 rms_eps = 1e-06
 group_eps = 1e-05
 rope_base = 10000.0
+
+
+def on_each_block(value, axis, dim, work, out_dim):
+    size, here, rows = (lax.axis_size(axis), lax.axis_index(axis), value.shape[dim])
+    right = [(i, (i + 1) % size) for i in range(size)]
+    behind = [(b, a) for a, b in right]
+    lower, upper = (lax.ppermute(value, axis, right), lax.ppermute(value, axis, behind))
+    made = work(value, here * rows)
+    length = made.shape[out_dim]
+    out = jnp.zeros((*made.shape[:out_dim], size * length, *made.shape[out_dim + 1 :]), made.dtype)
+
+    def put(out, made, holder):
+        return lax.dynamic_update_slice_in_dim(out, made, holder * length, axis=out_dim)
+
+    out = put(out, made, here)
+    for lap in range(1, size // 2 + 1):
+        below, above = ((here - lap) % size, (here + lap) % size)
+        block = (lower, upper)
+        if lap < size // 2:
+            lower, upper = (lax.ppermute(lower, axis, right), lax.ppermute(upper, axis, behind))
+        out = put(out, work(block[0], below * rows), below)
+        if 2 * lap < size:
+            out = put(out, work(block[1], above * rows), above)
+    return out
 
 
 def neutral_like(shard, identity):
@@ -125,11 +149,14 @@
         tok_f32 * lax.rsqrt(jnp.mean(tok_f32 * tok_f32, axis=-1, keepdims=True) + rms_eps) * in_gain
     ).astype(jnp.bfloat16)
     joined = jnp.concatenate([query_weight, key_weight, value_weight, gate_weight], axis=1)
-    projected = jnp.einsum(
-        "kux,xt->kut",
-        lax.all_gather(normed, "tp", axis=1, tiled=True),
-        joined,
-        preferred_element_type=jnp.float32,
+    projected = on_each_block(
+        normed,
+        "tp",
+        1,
+        lambda shard_2, at: jnp.einsum(
+            "kux,xt->kut", shard_2, joined, preferred_element_type=jnp.float32
+        ),
+        1,
     ).astype(jnp.bfloat16)
 
     def heads_of(columns):

time: 205 us -> 237 us (1.16)
  waiting for transfers between devices: 84.8 us -> 43.6 us
  local copies, waits for them, and re-layouts: 13.3 us -> 45 us
  matrix products: 27.4 us -> 51.4 us
  starting transfers between devices: 0.09 us -> 15.2 us
    all_gather x1 -> x0, waiting for transfers between devices: 53.8 us -> none  [body(): lax.all_gather(normed, 'tp', axis=1, tiled=True)]
    dynamic_update_slice x0 -> x8, local copies, waits for them, and re-layouts: none -> 26.6 us  [put(): lax.dynamic_update_slice_in_dim(out, made, holder * length, axis=out_dim)]
    dot_general x1 -> x8, matrix products: 9.51 us -> 25.2 us  [body(): jnp.einsum('kux,xt->kut', shard_2, joined, preferred_element_type=jnp.flo...]
    ppermute x0 -> x7, starting transfers between devices: none -> 15.1 us  [the longest x2 6.82 us: on_each_block(): lax.ppermute(upper, axis, behind)]
    ppermute x0 -> x7, waiting for transfers between devices: none -> 11.8 us  [the longest x1 11.1 us: on_each_block(): lax.ppermute(value, axis, right)]
    concatenate x8, local copies, waits for them, and re-layouts: 2.8 us -> 7.57 us  [rotate(): jnp.concatenate([first_half * cosine - second * sine_part, first_half * s...]
    dot_general x4, matrix products: 1.27 us -> 5.14 us  [advance(): jnp.einsum('shkd,shkv->shdv', k_scaled, v_block, preferred_element_type=j...]
    dot_general x4, matrix products: 1.33 us -> 5.19 us  [advance(): jnp.einsum('shqk,shkv->shqv', weights, v_block, preferred_element_type=jn...]
  transfers between devices with their start and end apart: 3 -> 9, of which waited for: 3 -> 4; matrix products, arithmetic and copies ran while one was open for 4% -> 23% of each run, Pallas kernels for 0% -> 0%
where the time goes in v1:
time: 237 us; the launch traced here: 235 us
  matrix products  51.4 us (22%)
  local copies, waits for them, and re-layouts  45 us (19%)
  waiting for transfers between devices  43.6 us (18%)
  blocking collectives  39 us (16%)
  other arithmetic  22.7 us (10%)
  between operations  18.4 us (8%)
  starting transfers between devices  15.2 us (6%)
    all_gather x2, waiting for transfers between devices, entering(): pieces = jax.tree.map(lambda part: lax.all_gather(part, axis), running)  31.8 us
    dynamic_update_slice x8, local copies, waits for them, and re-layouts, put(): lax.dynamic_update_slice_in_dim(out, made, holder * length, axis=out_dim)  26.6 us
    dot_general x8, matrix products, body(): jnp.einsum('kux,xt->kut', shard_2, joined, preferred_element_type=jnp.flo...  25.2 us
    unnamed x2, blocking collectives  20.7 us
    all_to_all x1, blocking collectives, body(): lax.all_to_all(gated, 'tp', split_axis=1, concat_axis=2, tiled=True)  18.3 us
    ppermute x1, waiting for transfers between devices, on_each_block(): lax.ppermute(value, axis, right)  11.1 us
    dot_general x1, matrix products, read_out(): jnp.einsum('shld,shdv->shlv', queries.astype(jnp.float32) * read_scale, c...  8.53 us
    concatenate x8, local copies, waits for them, and re-layouts, rotate(): jnp.concatenate([first_half * cosine - second * sine_part, first_half * s...  7.57 us
  transfers between devices with their start and end apart: 9, of which 4 were waited for; matrix products, arithmetic and copies ran while one was open for 23% of the time, Pallas kernels for 0%

profile of v1, /device:TPU:1, one launch (start us, length us, event | category | flops | bytes accessed | tf_op | source)
XLA Modules:
  0.0 235.4 jit_solution(9119376822354365042)
XLA Ops:
  9.7 2.6 %collective-permute-start = (bf16[4,64,2048]{2,1,0:T(8,128)(2,1)S(1)}, bf16[4,64,2048]{2,1,0:T(8,128)(2,1)}, u32[]{:S(2)}, u32[]{:S(2)}) collective-permute-start(bf16[4,64,2048]{2,1,0:T(8,128)(2,1)S(1)} %fusion.46), channel_id=1, source_target_pairs={{0,1},{1,2},{2,3},{3,4},{4,5},{5,6},{6,7},{7,0},{8,9},{9,10},{10,1... | collective-permute-start | bytes 3145736 | tf_op jit(solution)/shard_map/ppermute | solution.py:20
  13.0 11.1 %collective-permute-done = bf16[4,64,2048]{2,1,0:T(8,128)(2,1)} collective-permute-done((bf16[4,64,2048]{2,1,0:T(8,128)(2,1)S(1)}, bf16[4,64,2048]{2,1,0:T(8,128)(2,1)}, u32[]{:S(2)}, u32[]{:S(2)}) %collective-permute-start) | collective-permute-done | bytes 1048608 | tf_op jit(solution)/shard_map/ppermute | solution.py:20
  27.4 3.1 %fusion.125 = bf16[4,64,512]{1,2,0:T(8,128)(2,1)} fusion(bf16[4,64,2048]{2,1,0:T(8,128)(2,1)S(1)} %fusion.46, bf16[2048,128]{1,0:T(8,128)(2,1)S(1)} %copy-done.6, bf16[2048,128]{1,0:T(8,128)(2,1)S(1)} %copy-done.8, bf16[2048,128]{1,0:T(8,128)(2,1)S(1)} %copy-done.10, bf16[2048,128]{1,0:T(8,128)(2,1)} %param.14), kind=kOutput, calls=%fused_computation.172 | convolution fusion | flops 545259520 | bytes 3407872 | tf_op jit(solution)/shard_map/kux,xt->kut/dot_general | solution.py:156
  30.7 5.9 %dynamic_update_slice.28 = bf16[4,512,512]{1,2,0:T(8,128)(2,1)S(1)} dynamic-update-slice(bf16[4,512,512]{1,2,0:T(8,128)(2,1)S(1)} %broadcast_in_dim.10, bf16[4,64,512]{1,2,0:T(8,128)(2,1)} %fusion.125, s32[]{:T(128)} %constant.96.clone.1, s32[]{:T(128)S(6)} %select_n.211, s32[]{:T(128)} %constant.96.clone.1) | dynamic-update-slice | bytes 524292 | tf_op jit(solution)/shard_map/dynamic_update_slice | solution.py:26
  41.2 3.1 %fusion.124 = bf16[4,64,512]{1,2,0:T(8,128)(2,1)S(1)} fusion(bf16[4,64,2048]{2,1,0:T(8,128)(2,1)} %collective-permute-done, bf16[2048,128]{1,0:T(8,128)(2,1)} %param.17, bf16[2048,128]{1,0:T(8,128)(2,1)} %param.16, bf16[2048,128]{1,0:T(8,128)(2,1)} %param.15, bf16[2048,128]{1,0:T(8,128)(2,1)} %param.14), kind=kOutput, calls=%fused_computation.171 | convolution fusion | flops 545259520 | bytes 3407872 | tf_op jit(solution)/shard_map/kux,xt->kut/dot_general | solution.py:156
  46.3 3.1 %fusion.123 = bf16[4,64,512]{1,2,0:T(8,128)(2,1)S(1)} fusion(bf16[4,64,2048]{2,1,0:T(8,128)(2,1)} %collective-permute-done.1, bf16[2048,128]{1,0:T(8,128)(2,1)} %param.17, bf16[2048,128]{1,0:T(8,128)(2,1)} %param.16, bf16[2048,128]{1,0:T(8,128)(2,1)} %param.15, bf16[2048,128]{1,0:T(8,128)(2,1)} %param.14), kind=kOutput, calls=%fused_computation.170 | convolution fusion | flops 545259520 | bytes 3407872 | tf_op jit(solution)/shard_map/kux,xt->kut/dot_general | solution.py:156
  51.6 6.0 %collective-permute-start.5 = (bf16[4,64,2048]{2,1,0:T(8,128)(2,1)}, bf16[4,64,2048]{2,1,0:T(8,128)(2,1)}, u32[]{:S(2)}, u32[]{:S(2)}) collective-permute-start(bf16[4,64,2048]{2,1,0:T(8,128)(2,1)} %collective-permute-done.3), channel_id=1, source_target_pairs={{1,0},{2,1},{3,2},{4,3},{5,4},{6,5},{7,6},{0,7},{9,8},{10,9},{11,1... | collective-permute-start | bytes 3145736 | tf_op jit(solution)/shard_map/ppermute | solution.py:33
  57.6 3.1 %fusion.122 = bf16[4,64,512]{1,2,0:T(8,128)(2,1)S(1)} fusion(bf16[4,64,2048]{2,1,0:T(8,128)(2,1)} %collective-permute-done.2, bf16[2048,128]{1,0:T(8,128)(2,1)} %param.17, bf16[2048,128]{1,0:T(8,128)(2,1)} %param.16, bf16[2048,128]{1,0:T(8,128)(2,1)} %param.15, bf16[2048,128]{1,0:T(8,128)(2,1)} %param.14), kind=kOutput, calls=%fused_computation.169 | convolution fusion | flops 545259520 | bytes 3407872 | tf_op jit(solution)/shard_map/kux,xt->kut/dot_general | solution.py:156
  60.8 3.3 %fusion.121 = bf16[4,64,512]{1,2,0:T(8,128)(2,1)} fusion(bf16[4,64,2048]{2,1,0:T(8,128)(2,1)} %collective-permute-done.3, bf16[2048,128]{1,0:T(8,128)(2,1)S(1)} %copy-done.7, bf16[2048,128]{1,0:T(8,128)(2,1)S(1)} %copy-done.9, bf16[2048,128]{1,0:T(8,128)(2,1)S(1)} %copy-done.11, bf16[2048,128]{1,0:T(8,128)(2,1)S(1)} %copy-done.12), kind=kOutput, calls=%fused_computation.168 | convolution fusion | flops 545259520 | bytes 3407872 | tf_op jit(solution)/shard_map/kux,xt->kut/dot_general | solution.py:156
  64.1 3.3 %dynamic_update_slice.31 = bf16[4,512,512]{1,2,0:T(8,128)(2,1)S(1)} dynamic-update-slice(bf16[4,512,512]{1,2,0:T(8,128)(2,1)S(1)} %dynamic_update_slice.30, bf16[4,64,512]{1,2,0:T(8,128)(2,1)S(1)} %fusion.122, s32[]{:T(128)} %constant.96.clone.1, s32[]{:T(128)S(6)} %select_n.217, s32[]{:T(128)} %constant.96.clone.1) | dynamic-update-slice | bytes 524292 | tf_op jit(solution)/shard_map/dynamic_update_slice | solution.py:26
  67.5 5.7 %dynamic_update_slice.32 = bf16[4,512,512]{1,2,0:T(8,128)(2,1)S(1)} dynamic-update-slice(bf16[4,512,512]{1,2,0:T(8,128)(2,1)S(1)} %dynamic_update_slice.31, bf16[4,64,512]{1,2,0:T(8,128)(2,1)} %fusion.121, s32[]{:T(128)} %constant.96.clone.1, s32[]{:T(128)S(6)} %select_n.219, s32[]{:T(128)} %constant.96.clone.1) | dynamic-update-slice | bytes 524292 | tf_op jit(solution)/shard_map/dynamic_update_slice | solution.py:26
  73.2 3.1 %fusion.120 = bf16[4,64,512]{1,2,0:T(8,128)(2,1)S(1)} fusion(bf16[4,64,2048]{2,1,0:T(8,128)(2,1)} %collective-permute-done.4, bf16[2048,128]{1,0:T(8,128)(2,1)} %param.17, bf16[2048,128]{1,0:T(8,128)(2,1)} %param.16, bf16[2048,128]{1,0:T(8,128)(2,1)} %param.15, bf16[2048,128]{1,0:T(8,128)(2,1)} %param.14), kind=kOutput, calls=%fused_computation.167 | convolution fusion | flops 545259520 | bytes 3407872 | tf_op jit(solution)/shard_map/kux,xt->kut/dot_general | solution.py:156
  78.3 3.1 %fusion.119 = bf16[4,64,512]{1,2,0:T(8,128)(2,1)S(1)} fusion(bf16[4,64,2048]{2,1,0:T(8,128)(2,1)} %collective-permute-done.5, bf16[2048,128]{1,0:T(8,128)(2,1)} %param.17, bf16[2048,128]{1,0:T(8,128)(2,1)} %param.16, bf16[2048,128]{1,0:T(8,128)(2,1)} %param.15, bf16[2048,128]{1,0:T(8,128)(2,1)} %param.14), kind=kOutput, calls=%fused_computation.166 | convolution fusion | flops 545259520 | bytes 3407872 | tf_op jit(solution)/shard_map/kux,xt->kut/dot_general | solution.py:156
  83.4 3.1 %fusion.118 = bf16[4,64,512]{1,2,0:T(8,128)(2,1)S(1)} fusion(bf16[4,64,2048]{2,1,0:T(8,128)(2,1)} %collective-permute-done.6, bf16[2048,128]{1,0:T(8,128)(2,1)} %param.17, bf16[2048,128]{1,0:T(8,128)(2,1)} %param.16, bf16[2048,128]{1,0:T(8,128)(2,1)} %param.15, bf16[2048,128]{1,0:T(8,128)(2,1)} %param.14), kind=kOutput, calls=%fused_computation.165 | convolution fusion | flops 545259520 | bytes 3407872 | tf_op jit(solution)/shard_map/kux,xt->kut/dot_general | solution.py:156
  86.6 3.7 %dynamic_update_slice.35 = bf16[4,512,512]{1,2,0:T(8,128)(2,1)S(1)} dynamic-update-slice(bf16[4,512,512]{1,2,0:T(8,128)(2,1)S(1)} %dynamic_update_slice.34, bf16[4,64,512]{1,2,0:T(8,128)(2,1)S(1)} %fusion.118, s32[]{:T(128)} %constant.96.clone.1, s32[]{:T(128)S(6)} %select_n.225, s32[]{:T(128)} %constant.96.clone.1) | dynamic-update-slice | bytes 524292 | tf_op jit(solution)/shard_map/dynamic_update_slice | solution.py:26
  106.2 19.7 %while.15 = (s32[]{:T(128)}, f32[4,1,128,128]{3,2,0,1:T(8,128)S(1)}, f32[4,4,1,128,128]{4,3,1,2,0:T(8,128)}, f32[1]{0:T(128)}, bf16[4,4,1,128,128]{4,3,1,2,0:T(8...) while((s32[]{:T(128)}, ...), condition=%wide.region_2.3_spmd.clone.clone.clone, body=%wide.region_1.2_spmd.clone.clone.clone.sunk | while | flops 67977728 | bytes 2496632 | solution.py:104
  128.1 7.0 %all-reduce = f32[4]{0:T(128)S(1)} all-reduce(f32[4]{0:T(128)S(1)} %exponential_dynamic-update-slice_fusion), channel_id=2, replica_groups=mesh['sp_0'=8,'sp_1'=4,'tp'=8] {'sp_1'}, use_global_device_ids=true, to_apply=%add | all-reduce | flops 4 | bytes 32
  137.6 15.1 %all-gather.8.cloned.1.call-done = f32[16,1,128,128]{3,2,1,0:T(8,128)} async-done(((f32[4,1,128,128]{3,2,1,0:T(8,128)}), f32[16,1,128,128]{3,2,1,0:T(8,128)}) %all-gather.8.cloned.1.call-update) | async-done | bytes 1048592 | tf_op jit(solution)/shard_map/all_gather | solution.py:51
  152.7 3.9 %slice_add_fusion.8 = f32[4,1,128,128]{3,2,1,0:T(8,128)} fusion(f32[16,1,128,128]{3,2,1,0:T(8,128)} %all-gather.8.cloned.1.call-done, f32[]{:T(128)} %bitcast.20, f32[]{:T(128)} %bitcast.18, f32[16,1,128,128]{3,2,0,1:T(8,128)} %bitcast.209, f32[]{:T(128)} %bitcast.16, f32[]{:T(128)} %bitcast.13), kind=kLoop, calls=%fused_computation.101 | loop fusion | flops 458752 | bytes 1310736 | tf_op jit(solution)/shard_map/add | solution.py:116
  158.6 13.7 %all-reduce.1 = f32[8]{0:T(128)S(1)} all-reduce(f32[8]{0:T(128)S(1)} %dynamic-update-slice.1), channel_id=3, replica_groups=mesh['sp_0'=8,'sp_1'=4,'tp'=8] {'sp_0'}, use_global_device_ids=true, to_apply=%add.1 | all-reduce | flops 8 | bytes 64
  179.2 16.7 %all-gather.6.cloned.1.call-done = f32[8,4,1,128,128]{4,3,2,1,0:T(8,128)} async-done(((f32[1,4,1,128,128]{4,3,2,1,0:T(8,128)}), f32[8,4,1,128,128]{4,3,2,1,0:T(8,128)}) %all-gather.6.cloned.1.call-update) | async-done | bytes 2097168 | tf_op jit(solution)/shard_map/all_gather | solution.py:51
  195.9 8.5 %fusion.127 = (f32[4,512]{1,0:T(4,128)S(1)}, f32[4,512,128]{1,2,0:T(8,128)S(1)}) fusion(f32[4,512,128]{1,2,0:T(8,128)} %reshape.499, f32[8,4,1,128,128]{4,3,1,2,0:T(8,128)} %bitcast.216, f32[4,1,128,128]{3,2,1,0:T(8,128)S(1)} %copy-done.2, f32[16,1,128,128]{3,2,0,1:T(8,128)} %bitcast.210, f32[16,1,128,128]{3,2,1,0:T(8,128)} %all-gather.8.cloned.1.call-done, ...), kind=kOutput, calls=%fused_computation.174 | convolution fusion | flops 71170048 | bytes 5785608 | tf_op jit(solution)/shard_map/shld,shdv->shlv/dot_general | solution.py:125
  205.4 18.3 %all_to_all.18 = bf16[4,512,128]{2,0,1:T(4,128)(2,1)S(1)} all-to-all(bf16[4,512,128]{2,0,1:T(4,128)(2,1)S(1)} %copy.77), channel_id=1, replica_groups=mesh['sp_0'=8,'sp_1'=4,'tp'=8] {'tp'}, dimensions={1} | all-to-all | bytes 1048576 | tf_op jit(solution)/shard_map/all_to_all | solution.py:189
  223.7 3.6 %multiply_reduce_fusion = (f32[4,64]{1,0:T(4,128)S(1)}, f32[4,64,2048]{2,1,0:T(8,128)S(1)}) fusion(bf16[1024,2048]{1,0:T(8,128)(2,1)} %param.20, bf16[4,8,8,8,128]{4,3,2,1,0:T(8,128)(2,1)S(1)} %bitcast.215), kind=kOutput, calls=%fused_computation.51 | convolution fusion | flops 1074790144 | bytes 6816768 | tf_op jit(solution)/shard_map/hor,rn->hon/dot_general | solution.py:187
  (112 shorter events, 66.5 us)
Async XLA Ops:
  6.5 20.9 %copy-start.10 = (bf16[2048,128]{1,0:T(8,128)(2,1)S(1)}, bf16[2048,128]{1,0:T(8,128)(2,1)}, u32[]{:S(2)}) copy-start(bf16[2048,128]{1,0:T(8,128)(2,1)} %param.15) | copy-start | bytes 1572868
  6.5 20.9 %copy-start.8 = (bf16[2048,128]{1,0:T(8,128)(2,1)S(1)}, bf16[2048,128]{1,0:T(8,128)(2,1)}, u32[]{:S(2)}) copy-start(bf16[2048,128]{1,0:T(8,128)(2,1)} %param.16) | copy-start | bytes 1572868
  6.5 20.9 %copy-start.6 = (bf16[2048,128]{1,0:T(8,128)(2,1)S(1)}, bf16[2048,128]{1,0:T(8,128)(2,1)}, u32[]{:S(2)}) copy-start(bf16[2048,128]{1,0:T(8,128)(2,1)} %param.17) | copy-start | bytes 1572868
  6.5 146.2 %all-gather.8.cloned.1.call-start = ((), (), s32[]{:S(2)}) async-start(), calls=%async_computation.2 | async-start | bytes 1310720 | tf_op jit(solution)/shard_map/all_gather | solution.py:51
  9.7 14.3 %collective-permute-start = (bf16[4,64,2048]{2,1,0:T(8,128)(2,1)S(1)}, bf16[4,64,2048]{2,1,0:T(8,128)(2,1)}, u32[]{:S(2)}, u32[]{:S(2)}) collective-permute-start(bf16[4,64,2048]{2,1,0:T(8,128)(2,1)S(1)} %fusion.46), channel_id=1, source_target_pairs={{0,1},{1,2},{2,3},{3,4},{4,5},{5,6},{6,7},{7,0},{8,9},{9,10},{10,1... | collective-permute-start | bytes 3145736 | tf_op jit(solution)/shard_map/ppermute | solution.py:20
  12.3 24.4 %collective-permute-start.1 = (bf16[4,64,2048]{2,1,0:T(8,128)(2,1)S(1)}, bf16[4,64,2048]{2,1,0:T(8,128)(2,1)}, u32[]{:S(2)}, u32[]{:S(2)}) collective-permute-start(bf16[4,64,2048]{2,1,0:T(8,128)(2,1)S(1)} %fusion.46), channel_id=1, source_target_pairs={{1,0},{2,1},{3,2},{4,3},{5,4},{6,5},{7,6},{0,7},{9,8},{10,9},{11,1... | collective-permute-start | bytes 3145736 | tf_op jit(solution)/shard_map/ppermute | solution.py:20
  24.1 14.6 %collective-permute-start.2 = (bf16[4,64,2048]{2,1,0:T(8,128)(2,1)}, bf16[4,64,2048]{2,1,0:T(8,128)(2,1)}, u32[]{:S(2)}, u32[]{:S(2)}) collective-permute-start(bf16[4,64,2048]{2,1,0:T(8,128)(2,1)} %collective-permute-done), channel_id=1, source_target_pairs={{0,1},{1,2},{2,3},{3,4},{4,5},{5,6},{6,7},{7,0},{8,9},{9,10},{10,1... | collective-permute-start | bytes 3145736 | tf_op jit(solution)/shard_map/ppermute | solution.py:33
  36.7 14.9 %collective-permute-start.3 = (bf16[4,64,2048]{2,1,0:T(8,128)(2,1)}, bf16[4,64,2048]{2,1,0:T(8,128)(2,1)}, u32[]{:S(2)}, u32[]{:S(2)}) collective-permute-start(bf16[4,64,2048]{2,1,0:T(8,128)(2,1)} %collective-permute-done.1), channel_id=1, source_target_pairs={{1,0},{2,1},{3,2},{4,3},{5,4},{6,5},{7,6},{0,7},{9,8},{10,9},{11,1... | collective-permute-start | bytes 3145736 | tf_op jit(solution)/shard_map/ppermute | solution.py:33
  38.7 22.0 %collective-permute-start.4 = (bf16[4,64,2048]{2,1,0:T(8,128)(2,1)}, bf16[4,64,2048]{2,1,0:T(8,128)(2,1)}, u32[]{:S(2)}, u32[]{:S(2)}) collective-permute-start(bf16[4,64,2048]{2,1,0:T(8,128)(2,1)} %collective-permute-done.2), channel_id=1, source_target_pairs={{0,1},{1,2},{2,3},{3,4},{4,5},{5,6},{6,7},{7,0},{8,9},{9,10},{10,1... | collective-permute-start | bytes 3145736 | tf_op jit(solution)/shard_map/ppermute | solution.py:33
  51.5 9.3 %copy-start.7 = (bf16[2048,128]{1,0:T(8,128)(2,1)S(1)}, bf16[2048,128]{1,0:T(8,128)(2,1)}, u32[]{:S(2)}) copy-start(bf16[2048,128]{1,0:T(8,128)(2,1)} %param.17) | copy-start | bytes 1572868
  51.5 9.3 %copy-start.9 = (bf16[2048,128]{1,0:T(8,128)(2,1)S(1)}, bf16[2048,128]{1,0:T(8,128)(2,1)}, u32[]{:S(2)}) copy-start(bf16[2048,128]{1,0:T(8,128)(2,1)} %param.16) | copy-start | bytes 1572868
  51.5 9.3 %copy-start.11 = (bf16[2048,128]{1,0:T(8,128)(2,1)S(1)}, bf16[2048,128]{1,0:T(8,128)(2,1)}, u32[]{:S(2)}) copy-start(bf16[2048,128]{1,0:T(8,128)(2,1)} %param.15) | copy-start | bytes 1572868
  51.5 9.3 %copy-start.12 = (bf16[2048,128]{1,0:T(8,128)(2,1)S(1)}, bf16[2048,128]{1,0:T(8,128)(2,1)}, u32[]{:S(2)}) copy-start(bf16[2048,128]{1,0:T(8,128)(2,1)} %param.14) | copy-start | bytes 1572868
  51.6 26.7 %collective-permute-start.5 = (bf16[4,64,2048]{2,1,0:T(8,128)(2,1)}, bf16[4,64,2048]{2,1,0:T(8,128)(2,1)}, u32[]{:S(2)}, u32[]{:S(2)}) collective-permute-start(bf16[4,64,2048]{2,1,0:T(8,128)(2,1)} %collective-permute-done.3), channel_id=1, source_target_pairs={{1,0},{2,1},{3,2},{4,3},{5,4},{6,5},{7,6},{0,7},{9,8},{10,9},{11,1... | collective-permute-start | bytes 3145736 | tf_op jit(solution)/shard_map/ppermute | solution.py:33
  60.7 22.7 %collective-permute-start.6 = (bf16[4,64,2048]{2,1,0:T(8,128)(2,1)}, bf16[4,64,2048]{2,1,0:T(8,128)(2,1)}, u32[]{:S(2)}, u32[]{:S(2)}) collective-permute-start(bf16[4,64,2048]{2,1,0:T(8,128)(2,1)} %collective-permute-done.4), channel_id=1, source_target_pairs={{0,1},{1,2},{2,3},{3,4},{4,5},{5,6},{6,7},{7,0},{8,9},{9,10},{10,1... | collective-permute-start | bytes 3145736 | tf_op jit(solution)/shard_map/ppermute | solution.py:33
  92.5 2.5 %copy-start.3 = (bf16[4,1,512,64]{2,3,0,1:T(8,128)(2,1)}, bf16[4,1,512,64]{2,3,0,1:T(8,128)(2,1)S(1)}, u32[]{:S(2)}) copy-start(bf16[4,1,512,64]{2,3,0,1:T(8,128)(2,1)S(1)} %get-tuple-element.166) | copy-start | bytes 786436
  102.4 1.4 copy-start.1
  106.2 20.5 %copy-start.14 = (u32[256]{0:T(256)S(1)}, u32[256]{0:T(256)}, u32[]{:S(2)}) copy-start(u32[256]{0:T(256)} %constant.134) | copy-start | bytes 3076
  106.2 50.4 %copy-start.13 = (u32[256]{0:T(256)S(1)}, u32[256]{0:T(256)}, u32[]{:S(2)}) copy-start(u32[256]{0:T(256)} %constant.139) | copy-start | bytes 3076
  125.9 0.7 copy-start
  126.6 69.2 %all-gather.6.cloned.1.call-start = ((), (), s32[]{:S(2)}) async-start(), calls=%async_computation.1 | async-start | bytes 2359296 | tf_op jit(solution)/shard_map/all_gather | solution.py:51
  176.1 19.8 %copy-start.2 = (f32[4,1,128,128]{3,2,1,0:T(8,128)S(1)}, f32[4,1,128,128]{3,2,1,0:T(8,128)}, u32[]{:S(2)}) copy-start(f32[4,1,128,128]{3,2,1,0:T(8,128)} %slice_add_fusion.8) | copy-start | bytes 786436
  195.9 8.7 %copy-start.5 = (f32[128]{0:T(128)S(1)}, f32[128]{0:T(128)}, u32[]{:S(2)}) copy-start(f32[128]{0:T(128)} %param.19) | copy-start | bytes 1540
  223.7 3.6 %copy-start.4 = (f32[2048]{0:T(1024)S(1)}, f32[2048]{0:T(1024)}, u32[]{:S(2)}) copy-start(f32[2048]{0:T(1024)} %param.21) | copy-start | bytes 24580
Sparse Core Ops, SparseCore 0:
  126.8 25.9 all-gather.7
  156.8 39.0 all-gather.5
